TPU v7x, 32 devices: a whole 2x2x4 slice. The times are simulated.
32 devices in a mesh: sp: 8 (over z, x), tp: 4 (over y, core).
Axes of the slice: x: 2, y: 2, z: 4, core: 2. Of those that a mesh axis runs over, the one named last changes fastest.
Arguments:
- queries: bfloat16 [1024, 1024], P('sp', 'tp'), may hold values from -160 to 160
- keys: bfloat16 [1024, 256], P('sp', 'tp'), may hold values from -5 to 5
- values: bfloat16 [1024, 256], P('sp', 'tp'), may hold values from -6 to 6
- cum_gate: float32 [1024, 16], P('sp', 'tp'), as said below
- doc_ids: int32 [1024], P('sp'), may hold values from 0 to 7, never falling along the last dimension, each value on 1 to 640 neighbouring positions
- residual: bfloat16 [1024, 2048], P(('sp', 'tp')), may hold values from -6 to 6
- out_proj: bfloat16 [1024, 2048], replicated, may hold values from -0.1875 to 0.1875
- norm_gain: float32 [2048], replicated, may hold values from 0.1 to 1.9
- route_ids: int32 [1024, 2], P(('sp', 'tp')), may hold values from 0 to 7, all different within a row; in each aligned block of 32 rows (0 to 31, 32 to 63, ...) at most 16 rows name the same one
- route_weights: float32 [1024, 2], P(('sp', 'tp')), may hold values from 0.2 to 1
- expert_gate: bfloat16 [8, 2048, 1024], P('sp', None, 'tp'), may hold values from -0.125 to 0.125
- expert_up: bfloat16 [8, 2048, 1024], P('sp', None, 'tp'), may hold values from -0.125 to 0.125
- expert_down: bfloat16 [8, 1024, 2048], P('sp', 'tp'), may hold values from -0.1875 to 0.1875
Outputs:
- mixed: bfloat16 [1024, 2048], P(('sp', 'tp'))
Inputs may be any that keep to these rules, and one draw needn't show every extreme that they name: `route_ids`: within each aligned block of 32 rows no expert is named by more than 16 rows, and in every draw some block has an expert named by exactly 16 rows; the 2 experts of a row differ. `doc_ids`: never falling along positions; a document spans at most 640 positions, and one spans exactly that many. `cum_gate`: never rising along positions.
All inputs are finite; a program needn't handle non-finite values.
Results may differ from a plain program's by a relative error of at most 0.014.
Values may be sent and summed in bfloat16 or wider, within the bound.
A program may use at most 128 MiB of HBM per device.

v0:
```python
import jax
import jax.numpy as jnp
from jax import lax
from jax.sharding import PartitionSpec as P

D = 2048
HEAD_DIM = 64
TOP = 2
very_low = -1e30
norm_eps = 1e-06


def slot_ranks(picked_ids, experts):
    onehot = (picked_ids[..., None] == jnp.arange(experts, dtype=jnp.int32)).astype(jnp.int32)
    earlier = jnp.cumsum(onehot, axis=-2) - onehot
    return jnp.sum(earlier * onehot, axis=-1)


def local(
    queries,
    keys,
    values,
    cum_gate,
    doc_ids,
    residual,
    out_proj,
    norm_gain,
    route_ids,
    route_weights,
    expert_gate,
    expert_up,
    expert_down,
):
    own_tokens = queries.shape[0]
    head_count = queries.shape[1] // HEAD_DIM
    kv_count = keys.shape[1] // HEAD_DIM
    group_size = head_count // kv_count
    scale = HEAD_DIM ** (-0.5)
    own_start = lax.axis_index("sp") * own_tokens
    query_pos = own_start + jnp.arange(own_tokens, dtype=jnp.int32)
    query_heads = queries.reshape(own_tokens, kv_count, group_size, HEAD_DIM)
    query_gate = cum_gate.reshape(own_tokens, kv_count, group_size)
    gate_all, doc_all = (
        lax.all_gather(cum_gate, "sp", axis=0, tiled=True),
        lax.all_gather(doc_ids, "sp", axis=0, tiled=True),
    )

    def attend(state, key_block, value_block, first, block_len):
        gate_keys = lax.dynamic_slice_in_dim(gate_all, first, block_len, 0)
        doc_keys = lax.dynamic_slice_in_dim(doc_all, first, block_len, 0)
        key_heads = key_block.reshape(block_len, kv_count, HEAD_DIM)
        value_heads = value_block.reshape(block_len, kv_count, HEAD_DIM)
        scores = (
            jnp.einsum("tkgd,skd->tkgs", query_heads, key_heads, preferred_element_type=jnp.float32)
            * scale
        )
        scores = (
            scores
            + query_gate[..., None]
            - gate_keys.T.reshape(kv_count, group_size, block_len)[None]
        )
        key_pos = first + jnp.arange(block_len, dtype=jnp.int32)
        allowed = (key_pos[None, :] <= query_pos[:, None]) & (doc_keys[None, :] == doc_ids[:, None])
        allowed = allowed[:, None, None, :]
        scores = jnp.where(allowed, scores, very_low)
        top_old, total_old, summed_old = state
        top_new = jnp.maximum(top_old, jnp.max(scores, axis=-1))
        weights = jnp.where(allowed, jnp.exp(scores - top_new[..., None]), 0.0)
        fade = jnp.exp(top_old - top_new)
        total_new = total_old * fade + jnp.sum(weights, axis=-1)
        summed_new = summed_old * fade[..., None] + jnp.einsum(
            "tkgs,skd->tkgd",
            weights.astype(jnp.bfloat16),
            value_heads,
            preferred_element_type=jnp.float32,
        )
        return (top_new, total_new, summed_new)

    start_state = (
        jnp.full((own_tokens, kv_count, group_size), very_low, jnp.float32),
        jnp.zeros((own_tokens, kv_count, group_size), jnp.float32),
        jnp.zeros((own_tokens, kv_count, group_size, HEAD_DIM), jnp.float32),
    )
    key_piece = lax.all_gather(keys, "sp", axis=0, tiled=True)
    value_piece = lax.all_gather(values, "sp", axis=0, tiled=True)
    piece_len = key_piece.shape[0]
    block_len = min(piece_len, own_tokens)

    def one_block(index, inner):
        offset = index * block_len
        key_block = lax.dynamic_slice_in_dim(key_piece, offset, block_len, 0)
        value_block = lax.dynamic_slice_in_dim(value_piece, offset, block_len, 0)
        last_doc = lax.dynamic_index_in_dim(doc_all, offset + block_len - 1, 0, keepdims=False)
        needed = (offset <= own_start + own_tokens - 1) & (last_doc >= doc_ids[0])
        return lax.cond(
            needed,
            lambda carried: attend(carried, key_block, value_block, offset, block_len),
            lambda carried: carried,
            inner,
        )

    top, total, summed = lax.fori_loop(0, piece_len // block_len, one_block, start_state)
    attended = (
        (summed / total[..., None]).reshape(own_tokens, head_count * HEAD_DIM).astype(jnp.bfloat16)
    )
    sp_count = lax.axis_size("sp")
    rows_dev = residual.shape[0]
    plane_entries = lax.all_to_all(attended, "tp", split_axis=0, concat_axis=1, tiled=True)
    projected = jnp.dot(plane_entries, out_proj, preferred_element_type=jnp.float32)
    stream = (residual.astype(jnp.float32) + projected).astype(jnp.bfloat16)
    stream_f = stream.astype(jnp.float32)
    normed = stream_f * lax.rsqrt(jnp.mean(stream_f * stream_f, axis=1, keepdims=True) + norm_eps)
    normed = (normed * norm_gain[None, :]).astype(jnp.bfloat16)
    exp_dev = expert_gate.shape[0]
    experts = exp_dev * sp_count
    capacity = max(2, 2 * rows_dev * TOP // experts)
    own_flat = route_ids.reshape(-1)
    own_rank = slot_ranks(route_ids.reshape(1, rows_dev * TOP), experts)[0]
    own_dest = own_flat * capacity + own_rank
    row_of = jnp.arange(rows_dev * TOP, dtype=jnp.int32) // TOP
    outgoing = jnp.zeros((experts * capacity, D), jnp.bfloat16).at[own_dest].set(normed[row_of])
    arrived = lax.all_to_all(
        outgoing.reshape(experts, capacity, D), "sp", split_axis=0, concat_axis=1, tiled=True
    )
    arrived = arrived.reshape(exp_dev, sp_count, 1, capacity, D)
    piece = lax.all_gather(arrived, "tp", axis=2, tiled=True)
    gate = jnp.einsum("esncd,edf->esncf", piece, expert_gate, preferred_element_type=jnp.float32)
    upper = jnp.einsum("esncd,edf->esncf", piece, expert_up, preferred_element_type=jnp.float32)
    hidden = (jax.nn.silu(gate) * upper).astype(jnp.bfloat16)
    partial_value = jnp.einsum(
        "esncf,efd->esncd", hidden, expert_down, preferred_element_type=jnp.float32
    )
    expert_sums = lax.psum_scatter(
        partial_value.astype(jnp.bfloat16), "tp", scatter_dimension=2, tiled=True
    )
    expert_out = expert_sums.reshape(exp_dev, sp_count * capacity, D)
    returned = lax.all_to_all(expert_out, "sp", split_axis=1, concat_axis=0, tiled=True)
    selected = returned.reshape(experts * capacity, D)[own_dest]
    weighted = selected.astype(jnp.float32).reshape(rows_dev, TOP, D) * route_weights[..., None]
    return (stream_f + jnp.sum(weighted, axis=1)).astype(jnp.bfloat16)


def solution(mesh):
    in_specs = (
        P("sp", "tp"),
        P("sp", "tp"),
        P("sp", "tp"),
        P("sp", "tp"),
        P("sp"),
        P(("sp", "tp"), None),
        P(),
        P(),
        P(("sp", "tp"), None),
        P(("sp", "tp"), None),
        P("sp", None, "tp"),
        P("sp", None, "tp"),
        P("sp", "tp", None),
    )
    out_specs = P(("sp", "tp"), None)
    return jax.shard_map(local, mesh=mesh, in_specs=in_specs, out_specs=out_specs, check_vma=False)
```

profile of v0, /device:TPU:0, one launch (start us, length us, event | category | flops | bytes accessed | tf_op | source)
XLA Modules:
  0.0 280.7 jit_solution(1329913075445038006)
XLA Ops:
  6.5 28.3 %all_gather.16 = bf16[1024,64]{0,1:T(8,128)(2,1)S(1)} all-gather(bf16[128,64]{0,1:T(8,128)(2,1)} %param.18), channel_id=1, replica_groups=mesh['sp'=8,'tp'=4] {'sp'}, dimensions={0}, use_global_device_ids=true | all-gather | bytes 147456 | tf_op jit(solution)/shard_map/all_gather | solution.py:84
  34.8 26.4 %all_gather.18 = bf16[1024,64]{0,1:T(8,128)(2,1)S(1)} all-gather(bf16[128,64]{0,1:T(8,128)(2,1)} %param.19), channel_id=1, replica_groups=mesh['sp'=8,'tp'=4] {'sp'}, dimensions={0}, use_global_device_ids=true | all-gather | bytes 147456 | tf_op jit(solution)/shard_map/all_gather | solution.py:85
  61.2 0.9 copy.35
  62.2 26.3 %all_gather.17 = f32[1024,4]{0,1:T(4,128)S(1)} all-gather(f32[128,4]{0,1:T(4,128)} %param.20), channel_id=1, replica_groups=mesh['sp'=8,'tp'=4] {'sp'}, dimensions={0}, use_global_device_ids=true | all-gather | bytes 18432 | tf_op jit(solution)/shard_map/all_gather | solution.py:44
  88.4 16.5 %all-gather.1 = s32[8,1,128]{2,1,0:T(1,128)S(1)} all-gather(s32[1,1,128]{2,1,0:T(1,128)} %bitcast.128), channel_id=1, replica_groups=mesh['sp'=8,'tp'=4] {'sp'}, dimensions={0}, use_global_device_ids=true | all-gather | bytes 4608 | tf_op jit(solution)/shard_map/all_gather | solution.py:45
  104.9 0.0 copy-start.3
  105.0 0.0 copy-start.1
  105.0 18.1 %while.23 = (s32[]{:T(128)}, f32[128,1,4]{0,2,1:T(4,128)S(1)}, f32[128,1,4]{0,2,1:T(4,128)S(1)}, f32[128,1,4,64]{0,3,2,1:T(8,128)S(1)}, s32[]{:T(128)}, /*index=...) while((s32[]{:T(128)}, f32[128,1,4]{0,2,1:T(4,128)S(1)}, ...), condition=%wide.region_5.6_spmd.clone, body=%wide.region_0.5_spmd.clone.sunk | while | flops 17614608 | bytes 1258975 | solution.py:102
  105.0 0.7 dynamic_slice.68
  106.9 2.1 conditional.3
  107.0 0.1 dynamic_slice.50
  107.1 0.8 compare_and_fusion
  107.8 0.9 fusion.47
  108.8 0.2 fusion.7
  109.0 0.1 fusion.9
  109.1 0.7 dynamic_slice.68
  111.1 0.7 dynamic_slice.68
  113.1 0.7 dynamic_slice.68
  115.1 0.7 dynamic_slice.68
  117.1 0.7 dynamic_slice.68
  119.1 0.7 dynamic_slice.68
  121.1 0.7 dynamic_slice.68
  123.1 0.1 copy.36
  123.3 0.8 convert_element_type.76
  124.1 3.3 %all-to-all-start = ((bf16[4,32,256]{2,1,0:T(8,128)(2,1)}), bf16[4,32,256]{2,1,0:T(8,128)(2,1)S(1)}, u32[]{:S(2)}, u32[]{:S(2)}) async-start(bf16[4,32,256]{2,1,0:T(8,128)(2,1)} %convert_element_type.76), calls=%async_computation | async-start | bytes 131072 | tf_op jit(solution)/shard_map/all_to_all | solution.py:108
  127.4 0.0 all-gather.4.cloned.1.call-start
  127.4 0.1 copy.39
  127.5 0.1 eq.47
  127.6 0.1 fusion.43
  127.7 0.1 reduce_window_sum.11
  127.8 0.2 select_reduce_fusion
  128.0 0.1 copy.38
  128.1 0.1 mul.107
  128.2 3.2 %all-to-all-done = bf16[4,32,256]{2,1,0:T(8,128)(2,1)S(1)} async-done(((bf16[4,32,256]{2,1,0:T(8,128)(2,1)}), bf16[4,32,256]{2,1,0:T(8,128)(2,1)S(1)}, u32[]{:S(2)}, u32[]{:S(2)}) %all-to-all-start) | async-done | bytes 65568 | tf_op jit(solution)/shard_map/all_to_all | solution.py:108
  131.5 0.0 copy-start.2
  131.5 3.1 %multiply_reduce_fusion.1 = (f32[32]{0:T(128)S(1)}, f32[32,2048]{1,0:T(8,128)S(1)}) fusion(bf16[32,1024]{1,0:T(8,128)(2,1)S(1)} %bitcast.124, bf16[1024,2048]{1,0:T(8,128)(2,1)} %param.23, bf16[32,2048]{1,0:T(8,128)(2,1)S(1)} %copy-done.1), kind=kOutput, calls=%fused_computation.58 | convolution fusion | flops 134610912 | bytes 4653184 | tf_op jit(solution)/shard_map/dot_general | solution.py:109
  134.6 0.0 copy-start.5
  134.6 0.1 multiply_convert_fusion
  134.7 2.0 scatter_custom_fusion
  136.7 25.9 %all_to_all.34 = bf16[8,16,2048]{2,1,0:T(8,128)(2,1)} all-to-all(bf16[8,16,2048]{2,1,0:T(8,128)(2,1)S(1)} %bitcast.121), channel_id=1, replica_groups=mesh['sp'=8,'tp'=4] {'sp'}, dimensions={0} | all-to-all | bytes 1048576 | tf_op jit(solution)/shard_map/all_to_all | solution.py:122
  162.6 0.0 all-gather.4.cloned.1.call-update
  162.7 0.0 all-reduce.3.cloned.1.call-start
  162.7 20.8 %all-gather.4.cloned.1.call-done = bf16[8,64,2048]{2,1,0:T(8,128)(2,1)} async-done(((bf16[8,16,2048]{2,1,0:T(8,128)(2,1)}), bf16[8,64,2048]{2,1,0:T(8,128)(2,1)}) %all-gather.4.cloned.1.call-update) | async-done | bytes 2097168 | tf_op jit(solution)/shard_map/all_gather | solution.py:126
  183.5 2.3 fusion.30
  185.8 5.5 %fusion.24 = bf16[1,8,4,16,2048]{4,3,2,1,0:T(8,128)(2,1)} fusion(bf16[1,256,2048]{2,1,0:T(8,128)(2,1)S(1)} %copy-done, bf16[8,4,16,2048]{3,2,1,0:T(8,128)(2,1)} %bitcast.132, bf16[1,2048,256]{2,1,0:T(8,128)(2,1)} %param.28, f32[8,4,16,256]{3,2,1,0:T(8,128)S(1)} %fusion.30), kind=kOutput, calls=%fused_computation.36 | convolution fusion | flops 1075576832 | bytes 6815744 | tf_op jit(solution)/shard_map/esncf,efd->esncd/dot_general | solution.py:130
  191.3 0.0 all-reduce.3.cloned.1.call-update
  191.3 0.6 copy-done.6
  191.9 0.6 dynamic-slice
  192.5 50.3 %all-reduce.3.cloned.1.call-done = bf16[1,8,4,16,2048]{4,3,2,1,0:T(8,128)(2,1)} async-done(((bf16[1,8,4,16,2048]{4,3,2,1,0:T(8,128)(2,1)}), bf16[1,8,4,16,2048]{4,3,2,1,0:T(8,128)(2,1)}) %all-reduce.3.cloned.1.call-update) | async-done | bytes 2097168
  242.8 1.7 constant_dynamic-slice_fusion
  244.6 0.8 copy.53
  245.4 0.0 copy-start.4
  245.4 0.5 broadcast.235
  245.9 3.7 %reduce.9 = bf16[128,2048]{1,0:T(8,128)(2,1)S(1)} reduce(bf16[128,1,2048]{2,1,0:T(2,128)(2,1)S(1)} %bitcast.119, bf16[]{:T(256)} %broadcast.235), dimensions={1}, to_apply=%bitcast.111.reduce_sub_computation | reduce | bytes 1048578
  249.6 1.2 reshape.400
  250.8 5.5 %all-to-all-start.2 = ((bf16[8,2,16384]{2,1,0:T(2,128)(2,1)}), bf16[8,2,16384]{2,1,0:T(2,128)(2,1)S(1)}, u32[]{:S(2)}, u32[]{:S(2)}) async-start(bf16[8,2,16384]{2,1,0:T(2,128)(2,1)} %reshape.400), calls=%async_computation.2 | async-start | bytes 1048576 | tf_op jit(solution)/shard_map/all_to_all | solution.py:137
  256.3 0.1 copy.41
  256.4 14.2 %all-to-all-done.2 = bf16[8,2,16384]{2,1,0:T(2,128)(2,1)S(1)} async-done(((bf16[8,2,16384]{2,1,0:T(2,128)(2,1)}), bf16[8,2,16384]{2,1,0:T(2,128)(2,1)S(1)}, u32[]{:S(2)}, u32[]{:S(2)}) %all-to-all-start.2) | async-done | bytes 524320 | tf_op jit(solution)/shard_map/all_to_all | solution.py:137
  270.6 0.5 reshape.401
  271.1 0.3 copy.52
  271.4 0.7 gather_fusion
  272.2 0.3 reshape.357
  272.5 0.7 multiply_reduce_fusion
  273.2 0.7 add_convert_fusion
  (39 shorter events, 0.3 us)
Async XLA Ops:
  6.5 179.3 %copy-start = (bf16[1,256,2048]{2,1,0:T(8,128)(2,1)S(1)}, bf16[1,256,2048]{2,1,0:T(8,128)(2,1)}, u32[]{:S(2)}) copy-start(bf16[1,256,2048]{2,1,0:T(8,128)(2,1)} %param.29) | copy-start | bytes 3145732
  104.9 22.5 %copy-start.3 = (s32[32,2]{0,1:T(2,128)S(1)}, s32[32,2]{0,1:T(2,128)}, u32[]{:S(2)}) copy-start(s32[32,2]{0,1:T(2,128)} %param.25) | copy-start | bytes 772
  105.0 26.5 %copy-start.1 = (bf16[32,2048]{1,0:T(8,128)(2,1)S(1)}, bf16[32,2048]{1,0:T(8,128)(2,1)}, u32[]{:S(2)}) copy-start(bf16[32,2048]{1,0:T(8,128)(2,1)} %param.22) | copy-start | bytes 393220
  124.1 7.4 %all-to-all-start = ((bf16[4,32,256]{2,1,0:T(8,128)(2,1)}), bf16[4,32,256]{2,1,0:T(8,128)(2,1)S(1)}, u32[]{:S(2)}, u32[]{:S(2)}) async-start(bf16[4,32,256]{2,1,0:T(8,128)(2,1)} %convert_element_type.76), calls=%async_computation | async-start | bytes 131072 | tf_op jit(solution)/shard_map/all_to_all | solution.py:108
  127.4 56.1 %all-gather.4.cloned.1.call-start = ((), (), s32[]{:S(2)}) async-start(), calls=%async_computation.3 | async-start | bytes 2621440 | tf_op jit(solution)/shard_map/all_gather | solution.py:126
  131.5 3.2 %copy-start.2 = (f32[2048]{0:T(1024)S(1)}, f32[2048]{0:T(1024)}, u32[]{:S(2)}) copy-start(f32[2048]{0:T(1024)} %param.24) | copy-start | bytes 24580
  134.6 48.9 %copy-start.5 = (bf16[1,2048,256]{2,1,0:T(8,128)(2,1)S(1)}, bf16[1,2048,256]{2,1,0:T(8,128)(2,1)}, u32[]{:S(2)}) copy-start(bf16[1,2048,256]{2,1,0:T(8,128)(2,1)} %param.27) | copy-start | bytes 3145732
  162.7 80.2 %all-reduce.3.cloned.1.call-start = ((), (), s32[]{:S(2)}) async-start(), calls=%async_computation.4 | async-start | bytes 4194304
  191.3 0.7 copy-start.6
  245.4 10.9 %copy-start.4 = (f32[32,2]{0,1:T(2,128)S(1)}, f32[32,2]{0,1:T(2,128)}, u32[]{:S(2)}) copy-start(f32[32,2]{0,1:T(2,128)} %param.26) | copy-start | bytes 772
  250.8 19.8 %all-to-all-start.2 = ((bf16[8,2,16384]{2,1,0:T(2,128)(2,1)}), bf16[8,2,16384]{2,1,0:T(2,128)(2,1)S(1)}, u32[]{:S(2)}, u32[]{:S(2)}) async-start(bf16[8,2,16384]{2,1,0:T(2,128)(2,1)} %reshape.400), calls=%async_computation.2 | async-start | bytes 1048576 | tf_op jit(solution)/shard_map/all_to_all | solution.py:137
Sparse Core Ops, SparseCore 0:
  162.8 20.6 all-gather.3
  191.4 51.3 all-reduce.2
where the time goes:
time: 282 us; the launch traced here: 281 us
  blocking collectives  123 us (44%)
  waiting for transfers between devices  88.5 us (31%)
  local copies, waits for them, and re-layouts  17 us (6%)
  between operations  13.7 us (5%)
  matrix products  12 us (4%)
  loops' own time  10.9 us (4%)
  starting transfers between devices  8.88 us (3%)
  other arithmetic  6.46 us (2%)
    unnamed x3, waiting for transfers between devices  50.4 us
    all_gather x1, blocking collectives, local(): key_piece = lax.all_gather(keys, 'sp', axis=0, tiled=True)  28.3 us
    all_gather x1, blocking collectives, local(): value_piece = lax.all_gather(values, 'sp', axis=0, tiled=True)  26.4 us
    all_gather x1, blocking collectives, local(): lax.all_gather(cum_gate, 'sp', axis=0, tiled=True)  26.3 us
    all_to_all x1, blocking collectives, local(): lax.all_to_all(outgoing.reshape(experts, capacity, D), 'sp', split_axis=0...  25.9 us
    all_gather x1, waiting for transfers between devices, local(): piece = lax.all_gather(arrived, 'tp', axis=2, tiled=True)  20.8 us
    all_gather x1, blocking collectives, local(): lax.all_gather(doc_ids, 'sp', axis=0, tiled=True)  16.5 us
    all_to_all x1, waiting for transfers between devices, local(): lax.all_to_all(expert_out, 'sp', split_axis=1, concat_axis=0, tiled=True)  14.2 us
  transfers between devices with their start and end apart: 4, of which 4 were waited for; matrix products, arithmetic and copies ran while one was open for 1% of the time, Pallas kernels for 0%

commit v1 on v0

--- a/solution.py
+++ b/solution.py
@@ -1,3 +1,4 @@
+import functools
 import jax
 import jax.numpy as jnp
 from jax import lax
@@ -8,6 +9,17 @@
 TOP = 2
 very_low = -1e30
 norm_eps = 1e-06
+
+
+def hold_vector(arr, link_axis, array_axis, join_dim):
+    f_now = lax.axis_size(link_axis)
+    all_rows = jnp.split(arr, f_now, array_axis)
+    d_next = jnp.stack(all_rows, 0)
+    a_now = lax.all_to_all(d_next, axis_name=link_axis, split_axis=0, concat_axis=0)
+    return jnp.concatenate(a_now, join_dim)
+
+
+spot_rest = functools.partial(hold_vector, link_axis="sp", array_axis=1, join_dim=0)
 
 
 def slot_ranks(picked_ids, experts):
@@ -134,7 +146,7 @@
         partial_value.astype(jnp.bfloat16), "tp", scatter_dimension=2, tiled=True
     )
     expert_out = expert_sums.reshape(exp_dev, sp_count * capacity, D)
-    returned = lax.all_to_all(expert_out, "sp", split_axis=1, concat_axis=0, tiled=True)
+    returned = spot_rest(expert_out)
     selected = returned.reshape(experts * capacity, D)[own_dest]
     weighted = selected.astype(jnp.float32).reshape(rows_dev, TOP, D) * route_weights[..., None]
     return (stream_f + jnp.sum(weighted, axis=1)).astype(jnp.bfloat16)

time: 282 us -> 278 us (0.986)
  other arithmetic: 6.46 us -> 2.75 us
    unnamed x1 -> x0, other arithmetic: 3.7 us -> none
    unnamed x23 -> x26, local copies, waits for them, and re-layouts: 6.6 us -> 8.49 us
where the time goes in v1:
time: 278 us
  blocking collectives  123 us (44%)
  waiting for transfers between devices  88.5 us (32%)
  local copies, waits for them, and re-layouts  18.2 us (7%)
  between operations  13.6 us (5%)
  matrix products  12 us (4%)
  loops' own time  10.3 us (4%)
  starting transfers between devices  8.88 us (3%)
    unnamed x3, waiting for transfers between devices  50.4 us
    all_gather x1, blocking collectives, local(): key_piece = lax.all_gather(keys, 'sp', axis=0, tiled=True)  28.3 us
    all_gather x1, blocking collectives, local(): value_piece = lax.all_gather(values, 'sp', axis=0, tiled=True)  26.4 us
    all_gather x1, blocking collectives, local(): lax.all_gather(cum_gate, 'sp', axis=0, tiled=True)  26.3 us
    all_to_all x1, blocking collectives, local(): lax.all_to_all(outgoing.reshape(experts, capacity, D), 'sp', split_axis=0...  25.9 us
    all_gather x1, waiting for transfers between devices, local(): piece = lax.all_gather(arrived, 'tp', axis=2, tiled=True)  20.8 us
    all_gather x1, blocking collectives, local(): lax.all_gather(doc_ids, 'sp', axis=0, tiled=True)  16.5 us
    all_to_all x1, waiting for transfers between devices, hold_vector(): lax.all_to_all(d_next, axis_name=link_axis, split_axis=0, concat_axis=0)  14.2 us
  transfers between devices with their start and end apart: 4, of which 4 were waited for; matrix products, arithmetic and copies ran while one was open for 1% of the time, Pallas kernels for 0%

profile of v1, /device:TPU:0, one launch (start us, length us, event | category | flops | bytes accessed | tf_op | source)
XLA Modules:
  0.0 277.6 jit_solution(1128100446252790359)
XLA Ops:
  6.5 28.3 %all_gather.16 = bf16[1024,64]{0,1:T(8,128)(2,1)S(1)} all-gather(bf16[128,64]{0,1:T(8,128)(2,1)} %param.18), channel_id=1, replica_groups=mesh['sp'=8,'tp'=4] {'sp'}, dimensions={0}, use_global_device_ids=true | all-gather | bytes 147456 | tf_op jit(solution)/shard_map/all_gather | solution.py:96
  34.8 26.4 %all_gather.18 = bf16[1024,64]{0,1:T(8,128)(2,1)S(1)} all-gather(bf16[128,64]{0,1:T(8,128)(2,1)} %param.19), channel_id=1, replica_groups=mesh['sp'=8,'tp'=4] {'sp'}, dimensions={0}, use_global_device_ids=true | all-gather | bytes 147456 | tf_op jit(solution)/shard_map/all_gather | solution.py:97
  61.2 0.9 copy.41
  62.2 26.3 %all_gather.17 = f32[1024,4]{0,1:T(4,128)S(1)} all-gather(f32[128,4]{0,1:T(4,128)} %param.20), channel_id=1, replica_groups=mesh['sp'=8,'tp'=4] {'sp'}, dimensions={0}, use_global_device_ids=true | all-gather | bytes 18432 | tf_op jit(solution)/shard_map/all_gather | solution.py:56
  88.4 16.5 %all-gather.1 = s32[8,1,128]{2,1,0:T(1,128)S(1)} all-gather(s32[1,1,128]{2,1,0:T(1,128)} %bitcast.159), channel_id=1, replica_groups=mesh['sp'=8,'tp'=4] {'sp'}, dimensions={0}, use_global_device_ids=true | all-gather | bytes 4608 | tf_op jit(solution)/shard_map/all_gather | solution.py:57
  104.9 0.0 copy-start.3
  105.0 0.0 copy-start.1
  105.0 17.0 %while.23 = (s32[]{:T(128)}, f32[128,1,4]{0,2,1:T(4,128)S(1)}, f32[128,1,4]{0,2,1:T(4,128)S(1)}, f32[128,1,4,64]{0,3,2,1:T(8,128)S(1)}, s32[]{:T(128)}, /*index=...) while((s32[]{:T(128)}, f32[128,1,4]{0,2,1:T(4,128)S(1)}, ...), condition=%wide.region_5.6_spmd.clone, body=%wide.region_0.5_spmd.clone.sunk | while | flops 17614608 | bytes 1258975 | solution.py:114
  105.0 0.6 dynamic_slice.68
  106.8 2.1 conditional.3
  106.8 0.1 dynamic_slice.50
  106.9 0.8 compare_and_fusion
  107.7 0.9 fusion.55
  108.6 0.2 fusion.7
  108.8 0.1 fusion.9
  109.0 0.6 dynamic_slice.68
  110.8 0.6 dynamic_slice.68
  112.7 0.6 dynamic_slice.68
  114.6 0.6 dynamic_slice.68
  116.4 0.6 dynamic_slice.68
  118.3 0.6 dynamic_slice.68
  120.1 0.6 dynamic_slice.68
  122.0 0.1 copy.42
  122.1 0.8 convert_element_type.76
  122.9 3.3 %all-to-all-start = ((bf16[4,32,256]{2,1,0:T(8,128)(2,1)}), bf16[4,32,256]{2,1,0:T(8,128)(2,1)S(1)}, u32[]{:S(2)}, u32[]{:S(2)}) async-start(bf16[4,32,256]{2,1,0:T(8,128)(2,1)} %convert_element_type.76), calls=%async_computation | async-start | bytes 131072 | tf_op jit(solution)/shard_map/all_to_all | solution.py:120
  126.2 0.0 all-gather.4.cloned.1.call-start
  126.3 0.1 copy.45
  126.4 0.1 eq.47
  126.5 0.1 fusion.51
  126.6 0.1 reduce_window_sum.11
  126.7 0.2 select_reduce_fusion
  126.8 0.1 copy.44
  126.9 0.1 mul.107
  127.1 3.2 %all-to-all-done = bf16[4,32,256]{2,1,0:T(8,128)(2,1)S(1)} async-done(((bf16[4,32,256]{2,1,0:T(8,128)(2,1)}), bf16[4,32,256]{2,1,0:T(8,128)(2,1)S(1)}, u32[]{:S(2)}, u32[]{:S(2)}) %all-to-all-start) | async-done | bytes 65568 | tf_op jit(solution)/shard_map/all_to_all | solution.py:120
  130.3 3.1 %multiply_reduce_fusion.1 = (f32[32]{0:T(128)S(1)}, f32[32,2048]{1,0:T(8,128)S(1)}) fusion(bf16[32,1024]{1,0:T(8,128)(2,1)S(1)} %bitcast.155, bf16[1024,2048]{1,0:T(8,128)(2,1)} %param.23, bf16[32,2048]{1,0:T(8,128)(2,1)S(1)} %copy-done.1), kind=kOutput, calls=%fused_computation.57 | convolution fusion | flops 134610912 | bytes 4653184 | tf_op jit(solution)/shard_map/dot_general | solution.py:121
  133.5 0.0 copy-start.5
  133.5 0.1 multiply_convert_fusion
  133.6 2.0 scatter_custom_fusion
  135.6 25.9 %all_to_all.30 = bf16[8,16,2048]{2,1,0:T(8,128)(2,1)} all-to-all(bf16[8,16,2048]{2,1,0:T(8,128)(2,1)S(1)} %bitcast.152), channel_id=1, replica_groups=mesh['sp'=8,'tp'=4] {'sp'}, dimensions={0} | all-to-all | bytes 1048576 | tf_op jit(solution)/shard_map/all_to_all | solution.py:134
  161.5 0.0 all-gather.4.cloned.1.call-update
  161.5 0.0 all-reduce.3.cloned.1.call-start
  161.6 20.8 %all-gather.4.cloned.1.call-done = bf16[8,64,2048]{2,1,0:T(8,128)(2,1)} async-done(((bf16[8,16,2048]{2,1,0:T(8,128)(2,1)}), bf16[8,64,2048]{2,1,0:T(8,128)(2,1)}) %all-gather.4.cloned.1.call-update) | async-done | bytes 2097168 | tf_op jit(solution)/shard_map/all_gather | solution.py:138
  182.4 2.3 fusion.30
  184.7 5.5 %fusion.24 = bf16[1,8,4,16,2048]{4,3,2,1,0:T(8,128)(2,1)} fusion(bf16[1,256,2048]{2,1,0:T(8,128)(2,1)S(1)} %copy-done, bf16[8,4,16,2048]{3,2,1,0:T(8,128)(2,1)} %bitcast.163, bf16[1,2048,256]{2,1,0:T(8,128)(2,1)} %param.28, f32[8,4,16,256]{3,2,1,0:T(8,128)S(1)} %fusion.30), kind=kOutput, calls=%fused_computation.36 | convolution fusion | flops 1075576832 | bytes 6815744 | tf_op jit(solution)/shard_map/esncf,efd->esncd/dot_general | solution.py:142
  190.1 0.0 all-reduce.3.cloned.1.call-update
  190.2 0.6 copy-done.6
  190.8 0.6 dynamic-slice
  191.4 50.3 %all-reduce.3.cloned.1.call-done = bf16[1,8,4,16,2048]{4,3,2,1,0:T(8,128)(2,1)} async-done(((bf16[1,8,4,16,2048]{4,3,2,1,0:T(8,128)(2,1)}), bf16[1,8,4,16,2048]{4,3,2,1,0:T(8,128)(2,1)}) %all-reduce.3.cloned.1.call-update) | async-done | bytes 2097168
  241.7 1.7 constant_dynamic-slice_fusion
  243.4 0.6 fusion.50
  244.1 0.6 fusion.49
  244.7 0.6 fusion.48
  245.3 0.6 fusion.47
  245.9 0.6 fusion.46
  246.6 0.6 fusion.45
  247.2 0.6 fusion.44
  247.8 0.6 fusion.43
  248.5 5.5 %all-to-all-start.2 = ((bf16[8,1,16,2048]{3,2,1,0:T(8,128)(2,1)}), bf16[8,1,16,2048]{3,2,1,0:T(8,128)(2,1)S(1)}, u32[]{:S(2)}, u32[]{:S(2)}) async-start(bf16[8,1,16,2048]{3,2,1,0:T(8,128)(2,1)} %fusion.43), calls=%async_computation.2 | async-start | bytes 1048576 | tf_op jit(solution)/shard_map/all_to_all | solution.py:18
  254.0 0.1 copy.46
  254.1 14.2 %all-to-all-done.2 = bf16[8,1,16,2048]{3,2,1,0:T(8,128)(2,1)S(1)} async-done(((bf16[8,1,16,2048]{3,2,1,0:T(8,128)(2,1)}), bf16[8,1,16,2048]{3,2,1,0:T(8,128)(2,1)S(1)}, u32[]{:S(2)}, u32[]{:S(2)}) %all-to-all-start.2) | async-done | bytes 524320 | tf_op jit(solution)/shard_map/all_to_all | solution.py:18
  268.2 0.7 gather_fusion
  269.0 0.3 reshape.349
  269.3 0.7 multiply_reduce_fusion
  270.1 0.7 add_convert_fusion
  (41 shorter events, 0.3 us)
Async XLA Ops:
  6.5 178.1 %copy-start = (bf16[1,256,2048]{2,1,0:T(8,128)(2,1)S(1)}, bf16[1,256,2048]{2,1,0:T(8,128)(2,1)}, u32[]{:S(2)}) copy-start(bf16[1,256,2048]{2,1,0:T(8,128)(2,1)} %param.29) | copy-start | bytes 3145732
  104.9 21.3 %copy-start.3 = (s32[32,2]{0,1:T(2,128)S(1)}, s32[32,2]{0,1:T(2,128)}, u32[]{:S(2)}) copy-start(s32[32,2]{0,1:T(2,128)} %param.25) | copy-start | bytes 772
  105.0 25.4 %copy-start.1 = (bf16[32,2048]{1,0:T(8,128)(2,1)S(1)}, bf16[32,2048]{1,0:T(8,128)(2,1)}, u32[]{:S(2)}) copy-start(bf16[32,2048]{1,0:T(8,128)(2,1)} %param.22) | copy-start | bytes 393220
  122.9 7.4 %all-to-all-start = ((bf16[4,32,256]{2,1,0:T(8,128)(2,1)}), bf16[4,32,256]{2,1,0:T(8,128)(2,1)S(1)}, u32[]{:S(2)}, u32[]{:S(2)}) async-start(bf16[4,32,256]{2,1,0:T(8,128)(2,1)} %convert_element_type.76), calls=%async_computation | async-start | bytes 131072 | tf_op jit(solution)/shard_map/all_to_all | solution.py:120
  126.2 56.1 %all-gather.4.cloned.1.call-start = ((), (), s32[]{:S(2)}) async-start(), calls=%async_computation.3 | async-start | bytes 2621440 | tf_op jit(solution)/shard_map/all_gather | solution.py:138
  130.3 3.2 %copy-start.2 = (f32[2048]{0:T(1024)S(1)}, f32[2048]{0:T(1024)}, u32[]{:S(2)}) copy-start(f32[2048]{0:T(1024)} %param.24) | copy-start | bytes 24580
  133.5 48.9 %copy-start.5 = (bf16[1,2048,256]{2,1,0:T(8,128)(2,1)S(1)}, bf16[1,2048,256]{2,1,0:T(8,128)(2,1)}, u32[]{:S(2)}) copy-start(bf16[1,2048,256]{2,1,0:T(8,128)(2,1)} %param.27) | copy-start | bytes 3145732
  161.5 80.2 %all-reduce.3.cloned.1.call-start = ((), (), s32[]{:S(2)}) async-start(), calls=%async_computation.4 | async-start | bytes 4194304
  190.1 0.7 copy-start.6
  190.2 63.8 %copy-start.4 = (f32[32,2]{0,1:T(2,128)S(1)}, f32[32,2]{0,1:T(2,128)}, u32[]{:S(2)}) copy-start(f32[32,2]{0,1:T(2,128)} %param.26) | copy-start | bytes 772
  248.5 19.8 %all-to-all-start.2 = ((bf16[8,1,16,2048]{3,2,1,0:T(8,128)(2,1)}), bf16[8,1,16,2048]{3,2,1,0:T(8,128)(2,1)S(1)}, u32[]{:S(2)}, u32[]{:S(2)}) async-start(bf16[8,1,16,2048]{3,2,1,0:T(8,128)(2,1)} %fusion.43), calls=%async_computation.2 | async-start | bytes 1048576 | tf_op jit(solution)/shard_map/all_to_all | solution.py:18
Sparse Core Ops, SparseCore 0:
  161.6 20.6 all-gather.3
  190.3 51.3 all-reduce.2
